TPU v7x, 32 devices: a whole 2x2x4 slice. The times are simulated.
32 devices in a mesh: grp: 2 (over y), sp: 4 (over z), tp: 4 (over x, core).
Axes of the slice: x: 2, y: 2, z: 4, core: 2. Of those that a mesh axis runs over, the one named last changes fastest.
Arguments:
- tokens: bfloat16 [4096, 2, 2048], P(('grp', 'sp', 'tp')), parts along dimension 0, may hold values from -64 to 64
- w_query: bfloat16 [2048, 2048], P(None, 'tp'), may hold values from -0.21875 to 0.21875
- w_key: bfloat16 [2048, 2048], P(None, 'tp'), may hold values from -0.125 to 0.125
- w_value: bfloat16 [2048, 2048], P(None, 'tp'), may hold values from -0.125 to 0.125
- w_out: bfloat16 [2048, 2048], P('tp'), may hold values from -0.125 to 0.125
- head_lambda: float32 [16], P('tp'), may hold values from 0.3 to 0.8
- sub_gain: float32 [128], replicated, may hold values from 0.1 to 1.9
Outputs:
- mixed: bfloat16 [4096, 2, 2048], P(('grp', 'sp', 'tp')), parts along dimension 0
There are 2 independent parts, one for each index of `grp`. A program takes and returns all parts, laid end to end along the dimension named above; an argument that names none is the same for every part. Nothing has to cross between parts.
All inputs are finite; a program needn't handle non-finite values.
Results may differ from a plain program's by a relative error of at most 0.015.
The roundings to bfloat16 on the way count: a program that leaves them out, or rounds other values in their place, can miss the bound.
Values may be sent and summed in bfloat16 or wider, within the bound.
A program may use at most 128 MiB of HBM per device.

v0:
```python
import math

import jax
import jax.numpy as jnp
from jax import lax
from jax.sharding import PartitionSpec as P

SPAN = 64


NEG_FILL = -1e30
EPS_NORM = 1e-06


def key_block(state_in, queries, query_pos, key_blk, value_blk, key_start):
    run_max, run_sum, run_acc = state_in
    blk_len = key_blk.shape[0]
    heads_here = queries.shape[1]
    head_dim = queries.shape[3]
    key_pos = key_start + jnp.arange(blk_len, dtype=jnp.int32)
    key_four = key_blk.reshape(blk_len, heads_here, 2, head_dim)
    scores = jnp.einsum("qhmd,khmd->mhqk", queries, key_four, preferred_element_type=jnp.float32)
    scores = scores * head_dim ** (-0.5)
    allowed = (key_pos // SPAN)[None, :] <= (query_pos // SPAN)[:, None]
    new_max = jnp.maximum(run_max, jnp.max(jnp.where(allowed, scores, NEG_FILL), axis=-1))
    expo_vals = jnp.where(allowed, jnp.exp(scores - new_max[..., None]), 0.0)
    factor = jnp.exp(run_max - new_max)
    run_sum = run_sum * factor + jnp.sum(expo_vals, axis=-1)
    value_three = value_blk.reshape(blk_len, heads_here, 2 * head_dim)
    mixed_vals = jnp.einsum(
        "mhqk,khe->mhqe",
        expo_vals.astype(jnp.bfloat16),
        value_three,
        preferred_element_type=jnp.float32,
    )
    run_acc = run_acc * factor[..., None] + mixed_vals
    return (new_max, run_sum, run_acc)


def guarded_block(state_in, queries, query_pos, key_blk, value_blk, key_start):
    last_pos = query_pos[-1]

    def compute(inner_state):
        return key_block(inner_state, queries, query_pos, key_blk, value_blk, key_start)

    def keep(inner_state):
        return inner_state

    return lax.cond(key_start <= last_pos, compute, keep, state_in)


def sequence_piece(state_in, queries, query_pos, key_part, value_part):
    length = key_part.shape[0]
    step_len = math.gcd(length, 512)
    step_count = length // step_len

    def one_step(step_index, inner_state):
        offset = step_index * step_len
        key_blk = lax.dynamic_slice_in_dim(key_part, offset, step_len, 0)
        value_blk = lax.dynamic_slice_in_dim(value_part, offset, step_len, 0)
        return guarded_block(inner_state, queries, query_pos, key_blk, value_blk, offset)

    return lax.fori_loop(0, step_count, one_step, state_in)


def normalize(attn, sub_gain):
    mean_sq = jnp.mean(attn * attn, axis=-1, keepdims=True)
    normed = (attn * lax.rsqrt(mean_sq + EPS_NORM) * sub_gain).astype(jnp.bfloat16)
    return jnp.transpose(normed, (1, 0, 2)).reshape(attn.shape[1], attn.shape[0] * attn.shape[2])


def on_device(tokens, w_query, w_key, w_value, w_out, head_lambda, sub_gain):
    tp_count = lax.axis_size("tp")
    tok_rows = tokens.shape[0] * tp_count
    seq_count = tokens.shape[1]
    heads_here = head_lambda.shape[0]
    head_dim = w_query.shape[1] // (2 * heads_here)
    value_dim = 2 * head_dim
    query_cols = w_query.shape[1]
    w_joined = jnp.concatenate([w_query, w_key, w_value], axis=1)
    joined = jnp.dot(
        lax.all_gather(tokens, "tp", axis=0, tiled=True),
        w_joined,
        preferred_element_type=jnp.float32,
    ).astype(jnp.bfloat16)
    query_flat = joined[:, :, :query_cols]
    keys_here = joined[:, :, query_cols : 2 * query_cols]
    values_here = joined[:, :, 2 * query_cols :]
    sp_index = lax.axis_index("sp")
    own_first = sp_index * tok_rows
    lam_col = head_lambda[:, None, None]

    def attend(query_sets, first_rows):
        positions = [first + jnp.arange(tok_rows, dtype=jnp.int32) for first in first_rows]
        query_four = [qset.reshape(tok_rows, heads_here, 2, head_dim) for qset in query_sets]
        start_one = (
            jnp.full((2, heads_here, tok_rows), NEG_FILL, jnp.float32),
            jnp.zeros((2, heads_here, tok_rows), jnp.float32),
            jnp.zeros((2, heads_here, tok_rows, value_dim), jnp.float32),
        )
        start_state = tuple((start_one for seq_index in range(seq_count)))
        key_part = lax.all_gather(keys_here, "sp", axis=0, tiled=True)
        value_part = lax.all_gather(values_here, "sp", axis=0, tiled=True)
        new_states = []
        for seq_index in range(seq_count):
            new_states.append(
                sequence_piece(
                    start_state[seq_index],
                    query_four[seq_index],
                    positions[seq_index],
                    key_part[:, seq_index],
                    value_part[:, seq_index],
                )
            )
        final_states = tuple(new_states)
        results = []
        for run_max, run_sum, run_acc in final_states:
            attn = run_acc[0] / run_sum[0][..., None] - lam_col * run_acc[1] / run_sum[1][..., None]
            results.append(normalize(attn, sub_gain))
        return results

    normed_list = attend(
        [query_flat[:, seq_index] for seq_index in range(seq_count)],
        [own_first for seq_index in range(seq_count)],
    )
    normed = jnp.stack(normed_list, axis=1)
    return lax.psum_scatter(
        jnp.dot(normed, w_out, preferred_element_type=jnp.float32).astype(jnp.bfloat16),
        "tp",
        scatter_dimension=0,
        tiled=True,
    )


def solution(mesh):
    return jax.shard_map(
        on_device,
        mesh=mesh,
        in_specs=(
            P(("grp", "sp", "tp"), None, None),
            P(None, "tp"),
            P(None, "tp"),
            P(None, "tp"),
            P("tp", None),
            P("tp"),
            P(),
        ),
        out_specs=P(("grp", "sp", "tp"), None, None),
        check_vma=False,
    )
```

profile of v0, /device:TPU:0, one launch (start us, length us, event | category | flops | bytes accessed | tf_op | source)
XLA Modules:
  0.0 373.5 jit_solution(4716763115918646867)
XLA Ops:
  6.5 2.7 copy.39
  9.3 4.0 %copy.36 = bf16[2048,512]{0,1:T(8,128)(2,1)} copy(bf16[2048,512]{1,0:T(8,128)(2,1)} %param.16) | data formatting | bytes 4194304 | tf_op args[1]
  13.3 4.0 %copy.37 = bf16[2048,512]{0,1:T(8,128)(2,1)} copy(bf16[2048,512]{1,0:T(8,128)(2,1)} %param.17) | data formatting | bytes 4194304 | tf_op args[2]
  17.3 4.1 %copy.38 = bf16[2048,512]{0,1:T(8,128)(2,1)} copy(bf16[2048,512]{1,0:T(8,128)(2,1)} %param.18) | data formatting | bytes 4194304 | tf_op args[3]
  21.4 25.2 %all-gather.4.cloned.1.call-done = bf16[512,2,2048]{2,0,1:T(8,128)(2,1)} async-done(((bf16[128,2,2048]{2,0,1:T(8,128)(2,1)}), bf16[512,2,2048]{2,0,1:T(8,128)(2,1)}) %all-gather.4.cloned.1.call-update) | async-done | bytes 4194320 | tf_op jit(solution)/shard_map/all_gather | solution.py:82
  46.6 10.8 %fusion.38 = bf16[512,2,1536]{0,2,1:T(8,128)(2,1)S(1)} fusion(bf16[512,2,2048]{2,0,1:T(8,128)(2,1)} %all-gather.4.cloned.1.call-done, bf16[2048,512]{0,1:T(8,128)(2,1)} %copy.38, bf16[2048,512]{0,1:T(8,128)(2,1)} %copy.37, bf16[2048,512]{0,1:T(8,128)(2,1)} %copy.36), kind=kOutput, calls=%fused_computation.74 | convolution fusion | flops 6462898176 | bytes 13631488 | tf_op jit(solution)/shard_map/dot_general | solution.py:81
  57.4 1.7 copy-done.5
  59.1 1.5 fusion.57
  62.9 78.6 %all-gather.6.cloned.1.call-done = bf16[2048,2,512]{0,2,1:T(8,128)(2,1)} async-done(((bf16[512,2,512]{0,2,1:T(8,128)(2,1)}), bf16[2048,2,512]{0,2,1:T(8,128)(2,1)}) %all-gather.6.cloned.1.call-update) | async-done | bytes 4194320 | tf_op jit(solution)/shard_map/all_gather | solution.py:102
  141.5 4.8 %slice_bitcast_fusion.3 = (bf16[2048,512]{0,1:T(8,128)(2,1)}, bf16[2048,512]{0,1:T(8,128)(2,1)}) fusion(bf16[2048,2,512]{0,2,1:T(8,128)(2,1)} %all-gather.6.cloned.1.call-done), kind=kLoop, calls=%fused_computation.78 | loop fusion | bytes 8388608 | tf_op jit(solution)/shard_map/squeeze | solution.py:111
  146.3 76.0 %all-gather.8.cloned.1.call-done = bf16[2048,2,512]{0,2,1:T(8,128)(2,1)} async-done(((bf16[512,2,512]{0,2,1:T(8,128)(2,1)}), bf16[2048,2,512]{0,2,1:T(8,128)(2,1)}) %all-gather.8.cloned.1.call-update) | async-done | bytes 4194320 | tf_op jit(solution)/shard_map/all_gather | solution.py:103
  222.3 4.8 %slice_bitcast_fusion.2 = (bf16[2048,512]{0,1:T(8,128)(2,1)}, bf16[2048,512]{0,1:T(8,128)(2,1)}) fusion(bf16[2048,2,512]{0,2,1:T(8,128)(2,1)} %all-gather.8.cloned.1.call-done), kind=kLoop, calls=%fused_computation.77 | loop fusion | bytes 8388608 | tf_op jit(solution)/shard_map/squeeze | solution.py:112
  227.2 1.5 broadcast_in_dim.64.clone.1
  228.7 13.6 %while.35 = (s32[]{:T(128)}, f32[2,4,512]{2,1,0:T(4,128)S(1)}, f32[2,4,512]{2,1,0:T(4,128)S(1)}, f32[2,4,512,128]{3,2,0,1:T(8,128)}, s32[512]{0:T(512)S(1)}, /*i...) while((s32[]{:T(128)}, f32[2,4,512]{2,1,0:T(4,128)S(1)}, ...), condition=%wide.region_12.13_spmd, body=%wide.region_7.12_spmd.sunk | while | flops 823418368 | bytes 50882912 | solution.py:63
  229.9 8.5 %conditional.5 = ((f32[2,4,512]{2,1,0:T(4,128)S(1)}, f32[2,4,512]{2,1,0:T(4,128)S(1)}, f32[2,4,512,128]{3,2,0,1:T(8,128)})) conditional(s32[]{:T(128)} %convert_element_type.61, (f32[2,4,512]{2,1,0:T(4,128)S(1)}, f32[2,4,512]{2,1,0:T(4,128)S(1)}, f32[2,4,512,128]{3,2,0,1:T(8,128)}) %tuple.117, (s32[]{:T(128)}, s32[512]{0:T(512)S(1)}, ...), branch_computations={%region_8.8_spmd, %region_9.0_spmd} | conditional | flops 823418368 | bytes 50882692 | solution.py:49
  229.9 1.3 constant_dynamic-slice_fusion.2
  231.5 1.5 fusion.16
  233.0 2.0 fusion.19
  235.0 2.0 bitcast_add_fusion.1
  237.1 1.3 copy-done.4
  242.2 1.6 broadcast_in_dim.64.clone
  243.8 13.6 %while.34 = (s32[]{:T(128)}, f32[2,4,512]{2,1,0:T(4,128)S(1)}, f32[2,4,512]{2,1,0:T(4,128)S(1)}, f32[2,4,512,128]{3,2,0,1:T(8,128)}, s32[512]{0:T(512)S(1)}, /*i...) while((s32[]{:T(128)}, f32[2,4,512]{2,1,0:T(4,128)S(1)}, ...), condition=%wide.region_5.6_spmd, body=%wide.region_0.5_spmd.sunk | while | flops 823418368 | bytes 50882912 | solution.py:63
  245.1 8.5 %conditional.4 = ((f32[2,4,512]{2,1,0:T(4,128)S(1)}, f32[2,4,512]{2,1,0:T(4,128)S(1)}, f32[2,4,512,128]{3,2,0,1:T(8,128)})) conditional(s32[]{:T(128)} %convert_element_type.60, (f32[2,4,512]{2,1,0:T(4,128)S(1)}, f32[2,4,512]{2,1,0:T(4,128)S(1)}, f32[2,4,512,128]{3,2,0,1:T(8,128)}) %tuple.114, (s32[]{:T(128)}, s32[512]{0:T(512)S(1)}, ...), branch_computations={%region_1.0_spmd, %region_2.4_spmd} | conditional | flops 823418368 | bytes 50882692 | solution.py:49
  245.1 1.3 constant_dynamic-slice_fusion
  246.6 1.5 fusion
  248.2 2.0 fusion.3
  250.2 2.0 bitcast_add_fusion
  252.2 1.4 copy-done.2
  257.5 4.0 %multiply_reduce_fusion.1 = (f32[4,512]{1,0:T(4,128)S(1)}, f32[4,512,128]{2,1,0:T(8,128)S(1)}, f32[4,512]{1,0:T(4,128)S(1)}, f32[4,512,128]{2,1,0:T(8,128)S(1)}) fusion(f32[4,512]{1,0:T(4,128)S(1)} %get-tuple-element.612, f32[4]{0:T(128)S(1)} %copy-done.6, f32[4,512]{1,0:T(4,128)S(1)} %get-tuple-element.611, f32[4,512]{1,0:T(4,128)S(1)} %get-tuple-element.614, ...), kind=kLoop, calls=%fused_computation.97 | loop fusion | flops 3141632 | bytes 6340624 | tf_op jit(solution)/shard_map/reduce_sum | solution.py:67
  264.5 5.3 %convolution_convert_fusion = bf16[512,2,2048]{2,0,1:T(8,128)(2,1)} fusion(bf16[512,2048]{1,0:T(8,128)(2,1)S(1)} %copy-done, bf16[512,1,512]{2,0,1:T(8,128)(2,1)S(1)} %stack_reshape.7, bf16[512,1,512]{2,0,1:T(8,128)(2,1)} %stack_reshape.6), kind=kOutput, calls=%fused_computation.73 | convolution fusion | flops 2150105088 | bytes 7340032 | tf_op jit(solution)/shard_map/dot_general | solution.py:128
  269.9 93.8 %reduce-scatter.2.cloned.1.call-done = bf16[128,2,2048]{2,0,1:T(8,128)(2,1)} async-done(((bf16[512,2,2048]{2,0,1:T(8,128)(2,1)}), bf16[128,2,2048]{2,0,1:T(8,128)(2,1)}) %reduce-scatter.2.cloned.1.call-update) | async-done | bytes 1048592 | tf_op jit(solution)/shard_map/reduce_scatter | solution.py:127
  363.7 3.3 copy.47
  (63 shorter events, 10.8 us)
Async XLA Ops:
  6.5 258.0 %copy-start = (bf16[512,2048]{1,0:T(8,128)(2,1)S(1)}, bf16[512,2048]{1,0:T(8,128)(2,1)}, u32[]{:S(2)}) copy-start(bf16[512,2048]{1,0:T(8,128)(2,1)} %param.19) | copy-start | bytes 6291460
  6.5 40.1 %all-gather.4.cloned.1.call-start = ((), (), s32[]{:S(2)}) async-start(), calls=%async_computation.1 | async-start | bytes 5242880 | tf_op jit(solution)/shard_map/all_gather | solution.py:82
  9.3 132.2 %all-gather.6.cloned.1.call-start = ((), (), s32[]{:S(2)}) async-start(), calls=%async_computation.2 | async-start | bytes 5242880 | tf_op jit(solution)/shard_map/all_gather | solution.py:102
  57.4 1.7 copy-start.5
  60.6 161.7 %all-gather.8.cloned.1.call-start = ((), (), s32[]{:S(2)}) async-start(), calls=%async_computation.3 | async-start | bytes 5242880 | tf_op jit(solution)/shard_map/all_gather | solution.py:103
  61.3 302.4 %reduce-scatter.2.cloned.1.call-start = ((), (), s32[]{:S(2)}) async-start(), calls=%async_computation.4 | async-start | bytes 5242880 | tf_op jit(solution)/shard_map/reduce_scatter | solution.py:127
  233.0 2.0 copy-start.3
  237.0 1.3 copy-start.4
  243.8 13.7 %copy-start.6 = (f32[4]{0:T(128)S(1)}, f32[4]{0:T(128)}, u32[]{:S(2)}) copy-start(f32[4]{0:T(128)} %param.20) | copy-start | bytes 52
  248.1 2.0 copy-start.1
  252.2 1.4 copy-start.2
  257.5 4.0 %copy-start.7 = (f32[128]{0:T(128)S(1)}, f32[128]{0:T(128)}, u32[]{:S(2)}) copy-start(f32[128]{0:T(128)} %param.21) | copy-start | bytes 1540
Sparse Core Ops, SparseCore 0:
  9.4 37.1 all-gather.3
  60.7 80.7 all-gather.5
  143.1 79.2 all-gather.7
  270.0 93.6 reduce-scatter.1
where the time goes:
time: 374 us
  waiting for transfers between devices  274 us (73%)
  local copies, waits for them, and re-layouts  47.4 us (13%)
  matrix products  23.2 us (6%)
  between operations  13.3 us (4%)
  other arithmetic  9.39 us (3%)
  loops' own time  5.57 us (1%)
    reduce_scatter x1, waiting for transfers between devices, on_device(): lax.psum_scatter(jnp.dot(normed, w_out, preferred_element_type=jnp.float3...  93.8 us
    all_gather x1, waiting for transfers between devices, attend(): key_part = lax.all_gather(keys_here, 'sp', axis=0, tiled=True)  78.6 us
    all_gather x1, waiting for transfers between devices, attend(): value_part = lax.all_gather(values_here, 'sp', axis=0, tiled=True)  76 us
    all_gather x1, waiting for transfers between devices, on_device(): lax.all_gather(tokens, 'tp', axis=0, tiled=True)  25.2 us
    unnamed x12, local copies, waits for them, and re-layouts  16.5 us
    dot_general x1, matrix products, on_device(): jnp.dot(lax.all_gather(tokens, 'tp', axis=0, tiled=True), w_joined, prefe...  10.8 us
  transfers between devices with their start and end apart: 4, of which 4 were waited for; matrix products, arithmetic and copies ran while one was open for 5% of the time, Pallas kernels for 0%

commit v1 on v0

--- a/solution.py
+++ b/solution.py
@@ -1,8 +1,11 @@
+import functools
 import math
 
 import jax
 import jax.numpy as jnp
 from jax import lax
+from jax.experimental import pallas as pl
+from jax.experimental.pallas import tpu as pltpu
 from jax.sharding import PartitionSpec as P
 
 SPAN = 64
@@ -132,9 +135,370 @@
     )
 
 
+LANES = 128
+LOG2E = 1.4426950408889634
+
+
+def remote(src, dst, send, recv, where):
+    return pltpu.make_async_remote_copy(
+        src_ref=src,
+        dst_ref=dst,
+        send_sem=send,
+        recv_sem=recv,
+        device_id=where,
+        device_id_type=pl.DeviceIdType.MESH,
+    )
+
+
+def layer_kernel(
+    n_sp, n_tp, tok_ref, wq_ref, wk_ref, wv_ref, wo_ref, lam_ref, gain_ref, out_ref,
+    tokbuf, wbuf, wfull, stage, recv, ostage, obuf,
+    tok_send, tok_recv, tok_local, w_sem, wo_send, wo_recv, wo_local,
+    x_send, x_recv, x_local, o_send, o_recv,
+):
+    z = lax.axis_index("sp")
+    t = lax.axis_index("tp")
+    n_x = n_tp // 2
+    x = t // 2
+    core = t % 2
+    partner = x * 2 + (1 - core)
+    seqs, rows, _ = tok_ref.shape
+    heads = n_sp
+    zrows = rows * n_tp
+    prow = 2 * rows
+    half = LANES // 2
+
+    w_copies = [
+        pltpu.make_async_copy(ref, wbuf.at[j], w_sem.at[j])
+        for j, ref in enumerate((wq_ref, wk_ref, wv_ref))
+    ]
+    for cp in w_copies:
+        cp.start()
+    wo_copy = pltpu.make_async_copy(wo_ref, wfull.at[t], wo_local.at[0])
+    wo_copy.start()
+    own_copies = [
+        pltpu.make_async_copy(tok_ref.at[s], tokbuf.at[s, t], tok_local.at[s]) for s in range(seqs)
+    ]
+    for cp in own_copies:
+        cp.start()
+
+    barrier = pltpu.get_barrier_semaphore()
+    for dz in range(n_sp):
+        for dt in range(n_tp):
+            if dz or dt:
+                pl.semaphore_signal(
+                    barrier,
+                    inc=1,
+                    device_id={"sp": (z + dz) % n_sp, "tp": (t + dt) % n_tp},
+                    device_id_type=pl.DeviceIdType.MESH,
+                )
+    pl.semaphore_wait(barrier, n_sp * n_tp - 1)
+
+    def tok_x(s, k):
+        return remote(
+            tok_ref.at[s], tokbuf.at[s, t], tok_send.at[s, k], tok_recv.at[s, k],
+            {"tp": ((x + k) % n_x) * 2 + core},
+        )
+
+    def tok_pair(s):
+        return remote(
+            tok_ref.at[s], tokbuf.at[s, t], tok_send.at[s, 0], tok_recv.at[s, 0], {"tp": partner}
+        )
+
+    def tok_forward(s, k):
+        r = ((x + n_x - k) % n_x) * 2 + core
+        return remote(
+            tokbuf.at[s, r], tokbuf.at[s, r], tok_send.at[s, n_x - 1 + k],
+            tok_recv.at[s, n_x - 1 + k], {"tp": partner},
+        )
+
+    def wo_x(k):
+        return remote(
+            wo_ref, wfull.at[t], wo_send.at[k], wo_recv.at[k], {"tp": ((x + k) % n_x) * 2 + core}
+        )
+
+    def wo_pair():
+        return remote(wo_ref, wfull.at[t], wo_send.at[0], wo_recv.at[0], {"tp": partner})
+
+    def wo_forward(k):
+        r = ((x + n_x - k) % n_x) * 2 + core
+        return remote(
+            wfull.at[r], wfull.at[r], wo_send.at[n_x - 1 + k], wo_recv.at[n_x - 1 + k],
+            {"tp": partner},
+        )
+
+    for s in range(seqs):
+        for k in range(1, n_x):
+            tok_x(s, k).start()
+        tok_pair(s).start()
+    for k in range(1, n_x):
+        wo_x(k).start()
+
+    def row_of(z_src, k):
+        xk = (x + n_x - k) % n_x
+        return pl.multiple_of(z_src * zrows + xk * prow, prow)
+
+    def x_copy(s, k, d):
+        zd = (z + d) % n_sp
+        return remote(
+            stage.at[s, k, zd], recv.at[s, :, pl.ds(row_of(z, k), prow), :],
+            x_send.at[s, k, d - 1], x_recv.at[s, k, d - 1], {"sp": zd},
+        )
+
+    def x_own(s, k):
+        return pltpu.make_async_copy(
+            stage.at[s, k, z], recv.at[s, :, pl.ds(row_of(z, k), prow), :], x_local.at[s, k]
+        )
+
+    def project(s, k):
+        xk = (x + n_x - k) % n_x
+        lhs = tokbuf.at[s, pl.ds(xk * 2, 2)]
+
+        def one(j, _):
+            got = jnp.dot(
+                lhs[...].reshape(prow, tokbuf.shape[3]), wbuf[j],
+                preferred_element_type=jnp.float32,
+            ).astype(jnp.bfloat16)
+            for h in range(heads):
+                stage[s, k, h, j] = got[:, h * LANES : (h + 1) * LANES]
+            return 0
+
+        lax.fori_loop(0, 3, one, 0)
+        for d in range(1, n_sp):
+            x_copy(s, k, d).start()
+        x_own(s, k).start()
+
+    for s in range(seqs):
+        own_copies[s].wait()
+        tok_pair(s).wait_recv()
+        if s == 0:
+            for cp in w_copies:
+                cp.wait()
+        project(s, 0)
+        for k in range(1, n_x):
+            tok_x(s, k).wait_recv()
+            tok_forward(s, k).start()
+        for k in range(1, n_x):
+            tok_forward(s, k).wait_recv()
+            project(s, k)
+    wo_pair().start()
+
+    lam = lam_ref[z]
+    gain = gain_ref[...]
+    scale = half ** (-0.5) * LOG2E
+    head_id = t * heads + z
+    head_cols = pl.ds(pl.multiple_of(head_id * LANES, LANES), LANES)
+    lane = lax.broadcasted_iota(jnp.int32, (zrows, LANES), 1)
+    first_map = lane < half
+
+    def o_copy(s, qi, dt):
+        td = (t + dt) % n_tp
+        src = ostage.at[s, qi, td]
+        return remote(
+            src, obuf.at[s, :, head_cols], o_send.at[s, qi, dt], o_recv.at[s, head_id],
+            {"sp": qi, "tp": td},
+        )
+
+    def o_own(s):
+        return pltpu.make_async_copy(
+            ostage.at[s, z, t], obuf.at[s, :, head_cols], o_recv.at[s, head_id]
+        )
+
+    def attend(s):
+        def key_step(start, qs, state, masked):
+            sl = pl.ds(start, zrows)
+            sc = lax.dot_general(
+                qs, recv[s, 1, sl, :], (((1,), (1,)), ((), ())),
+                preferred_element_type=jnp.float32,
+            )
+            if masked:
+                row = lax.broadcasted_iota(jnp.int32, sc.shape, 0) % zrows
+                col = lax.broadcasted_iota(jnp.int32, sc.shape, 1)
+                sc = jnp.where(col // SPAN <= row // SPAN, sc, NEG_FILL)
+            top = jnp.max(sc, axis=-1, keepdims=True)
+            if state is not None:
+                top = jnp.maximum(top, state[0])
+            ex = jnp.exp2((sc - top) * scale)
+            tot = jnp.sum(ex, axis=-1, keepdims=True)
+            acc = jnp.dot(
+                ex.astype(jnp.bfloat16), recv[s, 2, sl, :], preferred_element_type=jnp.float32
+            )
+            if state is not None:
+                factor = jnp.exp2((state[0] - top) * scale)
+                tot = tot + state[1] * factor
+                acc = acc + state[2] * factor
+            return top, tot, acc
+
+        def q_step(qi, _):
+            start = pl.multiple_of(qi * zrows, zrows)
+            q = recv[s, 0, pl.ds(start, zrows), :]
+            zero = jnp.zeros_like(q)
+            qs = jnp.concatenate(
+                [jnp.where(first_map, q, zero), jnp.where(first_map, zero, q)], axis=0
+            )
+            state = key_step(start, qs, None, True)
+
+            def full(kj, inner):
+                return key_step(pl.multiple_of(kj * zrows, zrows), qs, inner, False)
+
+            _, tot, acc = lax.fori_loop(0, qi, full, state)
+            attn = acc[:zrows] / tot[:zrows] - lam * acc[zrows:] / tot[zrows:]
+            mean_sq = jnp.mean(attn * attn, axis=-1, keepdims=True)
+            normed = (attn * lax.rsqrt(mean_sq + EPS_NORM) * gain).astype(jnp.bfloat16)
+            ostage[s, qi] = normed.reshape(n_tp, rows, LANES)
+            for dt in range(1, n_tp):
+                o_copy(s, qi, dt).start()
+
+            @pl.when(qi == z)
+            def _():
+                o_own(s).start()
+
+            @pl.when(qi != z)
+            def _():
+                o_copy(s, qi, 0).start()
+
+            return 0
+
+        lax.fori_loop(0, n_sp, q_step, 0)
+
+    def wait_x(s):
+        for k in range(n_x):
+            x_own(s, k).wait()
+            for d in range(1, n_sp):
+                zs = (z + n_sp - d) % n_sp
+                remote(
+                    stage.at[s, k, 0], recv.at[s, :, pl.ds(row_of(zs, k), prow), :],
+                    x_send.at[s, k, d - 1], x_recv.at[s, k, d - 1], {"sp": zs},
+                ).wait_recv()
+
+    def finish(s):
+        def one(g, _):
+            cols = pl.ds(pl.multiple_of(g * LANES, LANES), LANES)
+            pltpu.make_async_copy(
+                ostage.at[s, 0, 0], obuf.at[s, :, cols], o_recv.at[s, g]
+            ).wait()
+            return 0
+
+        lax.fori_loop(0, n_tp * heads, one, 0)
+        width = heads * LANES
+        total = jnp.zeros((rows, out_ref.shape[2]), jnp.float32)
+        for g in range(n_tp):
+            part = jnp.dot(
+                obuf[s, :, g * width : (g + 1) * width], wfull[g],
+                preferred_element_type=jnp.float32,
+            )
+            total = total + part.astype(jnp.bfloat16).astype(jnp.float32)
+        out_ref[s] = total.astype(out_ref.dtype)
+
+    for s in range(seqs):
+        wait_x(s)
+        if s == seqs - 1:
+            for k in range(1, n_x):
+                wo_x(k).wait_recv()
+                wo_forward(k).start()
+        attend(s)
+    wo_copy.wait()
+    wo_pair().wait_recv()
+    for k in range(1, n_x):
+        wo_forward(k).wait_recv()
+    for s in range(seqs):
+        finish(s)
+
+    for s in range(seqs):
+        tok_pair(s).wait_send()
+        for k in range(1, n_x):
+            tok_x(s, k).wait_send()
+            tok_forward(s, k).wait_send()
+        for k in range(n_x):
+            for d in range(1, n_sp):
+                x_copy(s, k, d).wait_send()
+
+        def sent(qi, _, s=s):
+            for dt in range(1, n_tp):
+                o_copy(s, qi, dt).wait_send()
+
+            @pl.when(qi != z)
+            def _():
+                o_copy(s, qi, 0).wait_send()
+
+            return 0
+
+        lax.fori_loop(0, n_sp, sent, 0)
+    wo_pair().wait_send()
+    for k in range(1, n_x):
+        wo_x(k).wait_send()
+        wo_forward(k).wait_send()
+
+
+def fused_device(n_sp, n_tp, tokens, w_query, w_key, w_value, w_out, head_lambda, sub_gain):
+    rows, seqs, width = tokens.shape
+    cols = w_query.shape[1]
+    n_x = n_tp // 2
+    heads = head_lambda.shape[0]
+    bf = jnp.bfloat16
+    dma = pltpu.SemaphoreType.DMA
+    any_spec = pl.BlockSpec(memory_space=pl.ANY)
+    vmem_spec = pl.BlockSpec(memory_space=pltpu.VMEM)
+    out = pl.pallas_call(
+        functools.partial(layer_kernel, n_sp, n_tp),
+        out_shape=jax.ShapeDtypeStruct((seqs, rows, w_out.shape[1]), bf),
+        in_specs=[
+            vmem_spec, any_spec, any_spec, any_spec, any_spec,
+            pl.BlockSpec(memory_space=pltpu.SMEM), vmem_spec,
+        ],
+        out_specs=vmem_spec,
+        scratch_shapes=[
+            pltpu.VMEM((seqs, n_tp, rows, width), bf),
+            pltpu.VMEM((3, width, cols), bf),
+            pltpu.VMEM((n_tp,) + w_out.shape, bf),
+            pltpu.VMEM((seqs, n_x, heads, 3, 2 * rows, LANES), bf),
+            pltpu.VMEM((seqs, 3, rows * n_tp * n_sp, LANES), bf),
+            pltpu.VMEM((seqs, n_sp, n_tp, rows, LANES), bf),
+            pltpu.VMEM((seqs, rows, n_tp * heads * LANES), bf),
+            dma((seqs, 2 * n_x)),
+            dma((seqs, 2 * n_x)),
+            dma((seqs,)),
+            dma((3,)),
+            dma((2 * n_x,)),
+            dma((2 * n_x,)),
+            dma((1,)),
+            dma((seqs, n_x, n_sp)),
+            dma((seqs, n_x, n_sp)),
+            dma((seqs, n_x)),
+            dma((seqs, n_sp, n_tp)),
+            dma((seqs, n_tp * heads)),
+        ],
+        compiler_params=pltpu.CompilerParams(
+            collective_id=0, has_side_effects=True, vmem_limit_bytes=58 * 2**20
+        ),
+    )(
+        jnp.transpose(tokens, (1, 0, 2)), w_query, w_key, w_value, w_out,
+        head_lambda, sub_gain.reshape(1, -1),
+    )
+    return jnp.transpose(out, (1, 0, 2))
+
+
+def layer(tokens, w_query, w_key, w_value, w_out, head_lambda, sub_gain):
+    args = (tokens, w_query, w_key, w_value, w_out, head_lambda, sub_gain)
+    n_sp, n_tp = lax.axis_size("sp"), lax.axis_size("tp")
+    heads = head_lambda.shape[0]
+    fits = (
+        heads == n_sp
+        and n_sp > 1
+        and n_tp % 2 == 0
+        and w_query.shape[1] == heads * LANES
+        and sub_gain.shape[0] == LANES
+        and tokens.shape[0] % 16 == 0
+        and (tokens.shape[0] * n_tp) % SPAN == 0
+    )
+    if fits:
+        return fused_device(n_sp, n_tp, *args)
+    return on_device(*args)
+
+
 def solution(mesh):
     return jax.shard_map(
-        on_device,
+        layer,
         mesh=mesh,
         in_specs=(
             P(("grp", "sp", "tp"), None, None),

time: 374 us -> 113 us (0.30)
  the two profiles are of different devices: /device:TPU:0 before, /device:TPU:24 now
where the time goes in v1:
time: 113 us
  Pallas kernels  107 us (95%)
  local copies, waits for them, and re-layouts  5.82 us (5%)
    pallas_call x1, Pallas kernels, fused_device(): pl.pallas_call(functools.partial(layer_kernel, n_sp, n_tp), out_shape=jax...  107 us
    transpose x1, local copies, waits for them, and re-layouts, fused_device(): return jnp.transpose(out, (1, 0, 2))  3.27 us
    unnamed x1, local copies, waits for them, and re-layouts  2.54 us

profile of v1, /device:TPU:24, one launch (start us, length us, event | category | flops | bytes accessed | tf_op | source)
XLA Modules:
  0.0 113.0 jit_solution(12248641607763047448)
XLA Ops:
  0.0 2.5 %copy.11 = bf16[128,2,2048]{2,0,1:T(8,128)(2,1)} copy(bf16[128,2,2048]{2,1,0:T(2,128)(2,1)} %param.7) | data formatting | bytes 2097152 | tf_op args[0]
  2.5 107.2 %shard_map.73 = bf16[2,128,2048]{2,1,0:T(8,128)(2,1)} custom-call(bf16[2,128,2048]{2,1,0:T(8,128)(2,1)} %bitcast.6, bf16[2048,512]{1,0:T(8,128)(2,1)} %wq_ref.1, bf16[2048,512]{1,0:T(8,128)(2,1)} %wk_ref.1, bf16[2048,512]{1,0:T(8,128)(2,1)} %wv_ref.1, bf16[512,2048]{1,0:T(8,128)(2,1)} %wo_ref.1, f32[4]{0:T(128)} %lam_ref.1, f32[1,128]{1,0:T(1,128)} %bitcast.7), custom_call_target="tpu_custom_call" | custom-call | tf_op jit(solution)/shard_map/pallas_call | solution.py:442
  109.8 3.3 %copy.9 = bf16[128,2,2048]{2,1,0:T(2,128)(2,1)} copy(bf16[128,2,2048]{2,0,1:T(8,128)(2,1)} %bitcast.5) | data formatting | bytes 2097152 | tf_op jit(solution)/shard_map/transpose | solution.py:478

commit v2 on v1

--- a/solution.py
+++ b/solution.py
@@ -151,12 +151,14 @@
 
 
 def layer_kernel(
-    n_sp, n_tp, tok_ref, wq_ref, wk_ref, wv_ref, wo_ref, lam_ref, gain_ref, out_ref,
-    tokbuf, wbuf, wfull, stage, recv, ostage, obuf,
+    n_grp, n_sp, n_tp, tok_ref, wq_ref, wk_ref, wv_ref, wo_ref, lam_ref, gain_ref, out_ref,
+    tokbuf, wbuf, wfull, stage, recv, kvx, ostage, olocal, obuf,
     tok_send, tok_recv, tok_local, w_sem, wo_send, wo_recv, wo_local,
-    x_send, x_recv, x_local, o_send, o_recv,
+    x_send, x_recv, q_send, q_recv, x_local, e_send, e_recv, o_send, ol_send, o_recv,
 ):
+    grp = lax.axis_index("grp")
     z = lax.axis_index("sp")
+    low = n_sp // 2
     t = lax.axis_index("tp")
     n_x = n_tp // 2
     x = t // 2
@@ -192,7 +194,12 @@
                     device_id={"sp": (z + dz) % n_sp, "tp": (t + dt) % n_tp},
                     device_id_type=pl.DeviceIdType.MESH,
                 )
-    pl.semaphore_wait(barrier, n_sp * n_tp - 1)
+    for e in range(1, n_grp):
+        pl.semaphore_signal(
+            barrier, inc=1, device_id={"grp": (grp + e) % n_grp},
+            device_id_type=pl.DeviceIdType.MESH,
+        )
+    pl.semaphore_wait(barrier, n_sp * n_tp + n_grp - 2)
 
     def tok_x(s, k):
         return remote(
@@ -212,20 +219,31 @@
             tok_recv.at[s, n_x - 1 + k], {"tp": partner},
         )
 
+    part_rows = wo_ref.shape[0] // n_grp
+
+    def part(e):
+        return pl.ds(pl.multiple_of(((grp + n_grp - e) % n_grp) * part_rows, part_rows), part_rows)
+
     def wo_x(k):
         return remote(
-            wo_ref, wfull.at[t], wo_send.at[k], wo_recv.at[k], {"tp": ((x + k) % n_x) * 2 + core}
+            wo_ref.at[part(0)], wfull.at[t, part(0)], wo_send.at[k, 0, 0], wo_recv.at[k, 0, 0],
+            {"tp": ((x + k) % n_x) * 2 + core},
         )
 
     def wo_pair():
-        return remote(wo_ref, wfull.at[t], wo_send.at[0], wo_recv.at[0], {"tp": partner})
-
-    def wo_forward(k):
-        r = ((x + n_x - k) % n_x) * 2 + core
-        return remote(
-            wfull.at[r], wfull.at[r], wo_send.at[n_x - 1 + k], wo_recv.at[n_x - 1 + k],
-            {"tp": partner},
-        )
+        return remote(
+            wo_ref, wfull.at[t], wo_send.at[0, 0, 0], wo_recv.at[0, 0, 0], {"tp": partner}
+        )
+
+    def wo_grp(k, e):
+        blk = wfull.at[((x + n_x - k) % n_x) * 2 + core, part(0)]
+        return remote(
+            blk, blk, wo_send.at[k, 0, e], wo_recv.at[k, 0, e], {"grp": (grp + e) % n_grp}
+        )
+
+    def wo_forward(k, e):
+        blk = wfull.at[((x + n_x - k) % n_x) * 2 + core, part(e)]
+        return remote(blk, blk, wo_send.at[k, 1, e], wo_recv.at[k, 1, e], {"tp": partner})
 
     for s in range(seqs):
         for k in range(1, n_x):
@@ -234,25 +252,46 @@
     for k in range(1, n_x):
         wo_x(k).start()
 
+    def x_of(k):
+        return (x + n_x - k) % n_x
+
     def row_of(z_src, k):
-        xk = (x + n_x - k) % n_x
-        return pl.multiple_of(z_src * zrows + xk * prow, prow)
-
-    def x_copy(s, k, d):
+        return pl.multiple_of(z_src * zrows + x_of(k) * prow, prow)
+
+    def stays(row_shard, home):
+        return (home != row_shard) & (
+            (row_shard == 0) | ((row_shard < low) & (home >= low))
+        )
+
+    def kv_copy(s, k, d):
         zd = (z + d) % n_sp
         return remote(
-            stage.at[s, k, zd], recv.at[s, :, pl.ds(row_of(z, k), prow), :],
+            stage.at[s, x_of(k), zd, pl.ds(1, 2)],
+            recv.at[s, pl.ds(1, 2), pl.ds(row_of(z, k), prow), :],
             x_send.at[s, k, d - 1], x_recv.at[s, k, d - 1], {"sp": zd},
+        )
+
+    def q_copy(s, k, d):
+        zd = (z + d) % n_sp
+        return remote(
+            stage.at[s, x_of(k), zd, 0], recv.at[s, 0, pl.ds(row_of(z, k), prow), :],
+            q_send.at[s, k, d - 1], q_recv.at[s, k, d - 1], {"sp": zd},
+        )
+
+    def extra_copy(s, k, i):
+        return remote(
+            stage.at[s, x_of(k), low + i, pl.ds(1, 2)], kvx.at[s, i, :, x_of(k)],
+            e_send.at[s, k, i], e_recv.at[s, k, i], {"sp": 1},
         )
 
     def x_own(s, k):
         return pltpu.make_async_copy(
-            stage.at[s, k, z], recv.at[s, :, pl.ds(row_of(z, k), prow), :], x_local.at[s, k]
+            stage.at[s, x_of(k), z], recv.at[s, :, pl.ds(row_of(z, k), prow), :],
+            x_local.at[s, k],
         )
 
     def project(s, k):
-        xk = (x + n_x - k) % n_x
-        lhs = tokbuf.at[s, pl.ds(xk * 2, 2)]
+        lhs = tokbuf.at[s, pl.ds(x_of(k) * 2, 2)]
 
         def one(j, _):
             got = jnp.dot(
@@ -260,12 +299,22 @@
                 preferred_element_type=jnp.float32,
             ).astype(jnp.bfloat16)
             for h in range(heads):
-                stage[s, k, h, j] = got[:, h * LANES : (h + 1) * LANES]
+                stage[s, x_of(k), h, j] = got[:, h * LANES : (h + 1) * LANES]
             return 0
 
         lax.fori_loop(0, 3, one, 0)
         for d in range(1, n_sp):
-            x_copy(s, k, d).start()
+            kv_copy(s, k, d).start()
+
+            @pl.when(jnp.logical_not(stays(z, (z + d) % n_sp)))
+            def _(d=d):
+                q_copy(s, k, d).start()
+
+        @pl.when(z == 0)
+        def _():
+            for i in range(heads - low):
+                extra_copy(s, k, i).start()
+
         x_own(s, k).start()
 
     for s in range(seqs):
@@ -283,7 +332,6 @@
             project(s, k)
     wo_pair().start()
 
-    lam = lam_ref[z]
     gain = gain_ref[...]
     scale = half ** (-0.5) * LOG2E
     head_id = t * heads + z
@@ -304,48 +352,54 @@
             ostage.at[s, z, t], obuf.at[s, :, head_cols], o_recv.at[s, head_id]
         )
 
+    def key_step(qs, keys, vals, state, masked):
+        sc = lax.dot_general(
+            qs, keys, (((1,), (1,)), ((), ())), preferred_element_type=jnp.float32
+        )
+        if masked:
+            row = lax.broadcasted_iota(jnp.int32, sc.shape, 0) % zrows
+            col = lax.broadcasted_iota(jnp.int32, sc.shape, 1)
+            sc = jnp.where(col // SPAN <= row // SPAN, sc, NEG_FILL)
+        top = jnp.max(sc, axis=-1, keepdims=True)
+        if state is not None:
+            top = jnp.maximum(top, state[0])
+        ex = jnp.exp2((sc - top) * scale)
+        tot = jnp.sum(ex, axis=-1, keepdims=True)
+        acc = jnp.dot(ex.astype(jnp.bfloat16), vals, preferred_element_type=jnp.float32)
+        if state is not None:
+            factor = jnp.exp2((state[0] - top) * scale)
+            tot = tot + state[1] * factor
+            acc = acc + state[2] * factor
+        return top, tot, acc
+
+    def both_maps(q):
+        zero = jnp.zeros_like(q)
+        return jnp.concatenate(
+            [jnp.where(first_map, q, zero), jnp.where(first_map, zero, q)], axis=0
+        )
+
+    def close(state, lam):
+        _, tot, acc = state
+        attn = acc[:zrows] / tot[:zrows] - lam * acc[zrows:] / tot[zrows:]
+        mean_sq = jnp.mean(attn * attn, axis=-1, keepdims=True)
+        normed = (attn * lax.rsqrt(mean_sq + EPS_NORM) * gain).astype(jnp.bfloat16)
+        return normed.reshape(n_tp, rows, LANES)
+
     def attend(s):
-        def key_step(start, qs, state, masked):
-            sl = pl.ds(start, zrows)
-            sc = lax.dot_general(
-                qs, recv[s, 1, sl, :], (((1,), (1,)), ((), ())),
-                preferred_element_type=jnp.float32,
-            )
-            if masked:
-                row = lax.broadcasted_iota(jnp.int32, sc.shape, 0) % zrows
-                col = lax.broadcasted_iota(jnp.int32, sc.shape, 1)
-                sc = jnp.where(col // SPAN <= row // SPAN, sc, NEG_FILL)
-            top = jnp.max(sc, axis=-1, keepdims=True)
-            if state is not None:
-                top = jnp.maximum(top, state[0])
-            ex = jnp.exp2((sc - top) * scale)
-            tot = jnp.sum(ex, axis=-1, keepdims=True)
-            acc = jnp.dot(
-                ex.astype(jnp.bfloat16), recv[s, 2, sl, :], preferred_element_type=jnp.float32
-            )
-            if state is not None:
-                factor = jnp.exp2((state[0] - top) * scale)
-                tot = tot + state[1] * factor
-                acc = acc + state[2] * factor
-            return top, tot, acc
-
-        def q_step(qi, _):
+        def q_step(step, _):
+            qi = n_sp - 1 - step
             start = pl.multiple_of(qi * zrows, zrows)
-            q = recv[s, 0, pl.ds(start, zrows), :]
-            zero = jnp.zeros_like(q)
-            qs = jnp.concatenate(
-                [jnp.where(first_map, q, zero), jnp.where(first_map, zero, q)], axis=0
-            )
-            state = key_step(start, qs, None, True)
+
+            def block(j, first):
+                return recv[s, j, pl.ds(pl.multiple_of(first, zrows), zrows), :]
+
+            qs = both_maps(block(0, start))
+            state = key_step(qs, block(1, start), block(2, start), None, True)
 
             def full(kj, inner):
-                return key_step(pl.multiple_of(kj * zrows, zrows), qs, inner, False)
-
-            _, tot, acc = lax.fori_loop(0, qi, full, state)
-            attn = acc[:zrows] / tot[:zrows] - lam * acc[zrows:] / tot[zrows:]
-            mean_sq = jnp.mean(attn * attn, axis=-1, keepdims=True)
-            normed = (attn * lax.rsqrt(mean_sq + EPS_NORM) * gain).astype(jnp.bfloat16)
-            ostage[s, qi] = normed.reshape(n_tp, rows, LANES)
+                return key_step(qs, block(1, kj * zrows), block(2, kj * zrows), inner, False)
+
+            ostage[s, qi] = close(lax.fori_loop(0, qi, full, state), lam_ref[z])
             for dt in range(1, n_tp):
                 o_copy(s, qi, dt).start()
 
@@ -359,17 +413,69 @@
 
             return 0
 
-        lax.fori_loop(0, n_sp, q_step, 0)
+        lax.fori_loop(0, n_sp - jnp.minimum(z, low), q_step, 0)
+
+    first_local = jnp.where(z < low, z + 1, heads)
+
+    def local_cols(h):
+        return pl.ds(pl.multiple_of((t * heads + h) * LANES, LANES), LANES)
+
+    def ol_copy(s, h, dt):
+        td = (t + dt) % n_tp
+        return remote(
+            olocal.at[s, h, td], obuf.at[s, :, local_cols(h)], ol_send.at[s, h, dt],
+            o_recv.at[s, t * heads + h], {"tp": td},
+        )
+
+    def ol_own(s, h):
+        return pltpu.make_async_copy(
+            olocal.at[s, h, t], obuf.at[s, :, local_cols(h)], o_recv.at[s, t * heads + h]
+        )
+
+    def attend_local(s):
+        @pl.when(z == 1)
+        def _():
+            for k in range(n_x):
+                for i in range(heads - low):
+                    extra_copy(s, k, i).wait_recv()
+
+        def h_step(h, _):
+            def own(j):
+                return stage[s, :, h, j].reshape(zrows, LANES)
+
+            qs = both_maps(own(0))
+            state = key_step(qs, own(1), own(2), None, True)
+
+            def before(i, inner):
+                keys = kvx[s, h - low, 0].reshape(zrows, LANES)
+                vals = kvx[s, h - low, 1].reshape(zrows, LANES)
+                return key_step(qs, keys, vals, inner, False)
+
+            olocal[s, h] = close(lax.fori_loop(0, z, before, state), lam_ref[h])
+            for dt in range(1, n_tp):
+                ol_copy(s, h, dt).start()
+            ol_own(s, h).start()
+            return 0
+
+        lax.fori_loop(first_local, heads, h_step, 0)
 
     def wait_x(s):
         for k in range(n_x):
             x_own(s, k).wait()
             for d in range(1, n_sp):
                 zs = (z + n_sp - d) % n_sp
+                at = pl.ds(row_of(zs, k), prow)
                 remote(
-                    stage.at[s, k, 0], recv.at[s, :, pl.ds(row_of(zs, k), prow), :],
+                    stage.at[s, 0, 0, pl.ds(1, 2)], recv.at[s, pl.ds(1, 2), at, :],
                     x_send.at[s, k, d - 1], x_recv.at[s, k, d - 1], {"sp": zs},
                 ).wait_recv()
+
+                @pl.when(jnp.logical_not(stays(zs, z)))
+                def _(k=k, d=d, zs=zs, at=at):
+                    remote(
+                        stage.at[s, 0, 0, 0], recv.at[s, 0, at, :],
+                        q_send.at[s, k, d - 1], q_recv.at[s, k, d - 1], {"sp": zs},
+                    ).wait_recv()
 
     def finish(s):
         def one(g, _):
@@ -391,16 +497,37 @@
         out_ref[s] = total.astype(out_ref.dtype)
 
     for s in range(seqs):
+        if s < seqs - 1:
+            attend_local(s)
+        else:
+
+            @pl.when(z == 0)
+            def _(s=s):
+                attend_local(s)
+
         wait_x(s)
         if s == seqs - 1:
             for k in range(1, n_x):
+                for e in range(1, n_grp):
+                    wo_grp(k, e).wait_recv()
+                    wo_forward(k, e).start()
+        attend(s)
+        if s == 0:
+            for k in range(1, n_x):
                 wo_x(k).wait_recv()
-                wo_forward(k).start()
-        attend(s)
+                for e in range(1, n_grp):
+                    wo_grp(k, e).start()
+                wo_forward(k, 0).start()
+
+    @pl.when(z != 0)
+    def _():
+        attend_local(seqs - 1)
+
     wo_copy.wait()
     wo_pair().wait_recv()
     for k in range(1, n_x):
-        wo_forward(k).wait_recv()
+        for e in range(n_grp):
+            wo_forward(k, e).wait_recv()
     for s in range(seqs):
         finish(s)
 
@@ -411,9 +538,19 @@
             tok_forward(s, k).wait_send()
         for k in range(n_x):
             for d in range(1, n_sp):
-                x_copy(s, k, d).wait_send()
-
-        def sent(qi, _, s=s):
+                kv_copy(s, k, d).wait_send()
+
+                @pl.when(jnp.logical_not(stays(z, (z + d) % n_sp)))
+                def _(s=s, k=k, d=d):
+                    q_copy(s, k, d).wait_send()
+
+            @pl.when(z == 0)
+            def _(s=s, k=k):
+                for i in range(heads - low):
+                    extra_copy(s, k, i).wait_send()
+
+        def sent(step, _, s=s):
+            qi = n_sp - 1 - step
             for dt in range(1, n_tp):
                 o_copy(s, qi, dt).wait_send()
 
@@ -423,14 +560,24 @@
 
             return 0
 
-        lax.fori_loop(0, n_sp, sent, 0)
+        lax.fori_loop(0, n_sp - jnp.minimum(z, low), sent, 0)
+
+        def local_sent(h, _, s=s):
+            for dt in range(1, n_tp):
+                ol_copy(s, h, dt).wait_send()
+            return 0
+
+        lax.fori_loop(first_local, heads, local_sent, 0)
     wo_pair().wait_send()
     for k in range(1, n_x):
         wo_x(k).wait_send()
-        wo_forward(k).wait_send()
-
-
-def fused_device(n_sp, n_tp, tokens, w_query, w_key, w_value, w_out, head_lambda, sub_gain):
+        for e in range(n_grp):
+            wo_forward(k, e).wait_send()
+            if e:
+                wo_grp(k, e).wait_send()
+
+
+def fused_device(n_grp, n_sp, n_tp, tokens, w_query, w_key, w_value, w_out, head_lambda, sub_gain):
     rows, seqs, width = tokens.shape
     cols = w_query.shape[1]
     n_x = n_tp // 2
@@ -440,7 +587,7 @@
     any_spec = pl.BlockSpec(memory_space=pl.ANY)
     vmem_spec = pl.BlockSpec(memory_space=pltpu.VMEM)
     out = pl.pallas_call(
-        functools.partial(layer_kernel, n_sp, n_tp),
+        functools.partial(layer_kernel, n_grp, n_sp, n_tp),
         out_shape=jax.ShapeDtypeStruct((seqs, rows, w_out.shape[1]), bf),
         in_specs=[
             vmem_spec, any_spec, any_spec, any_spec, any_spec,
@@ -453,19 +600,26 @@
             pltpu.VMEM((n_tp,) + w_out.shape, bf),
             pltpu.VMEM((seqs, n_x, heads, 3, 2 * rows, LANES), bf),
             pltpu.VMEM((seqs, 3, rows * n_tp * n_sp, LANES), bf),
+            pltpu.VMEM((seqs, heads - n_sp // 2, 2, n_x, 2 * rows, LANES), bf),
             pltpu.VMEM((seqs, n_sp, n_tp, rows, LANES), bf),
+            pltpu.VMEM((seqs, heads, n_tp, rows, LANES), bf),
             pltpu.VMEM((seqs, rows, n_tp * heads * LANES), bf),
             dma((seqs, 2 * n_x)),
             dma((seqs, 2 * n_x)),
             dma((seqs,)),
             dma((3,)),
-            dma((2 * n_x,)),
-            dma((2 * n_x,)),
+            dma((n_x, 2, n_grp)),
+            dma((n_x, 2, n_grp)),
             dma((1,)),
             dma((seqs, n_x, n_sp)),
             dma((seqs, n_x, n_sp)),
+            dma((seqs, n_x, n_sp)),
+            dma((seqs, n_x, n_sp)),
             dma((seqs, n_x)),
+            dma((seqs, n_x, heads)),
+            dma((seqs, n_x, heads)),
             dma((seqs, n_sp, n_tp)),
+            dma((seqs, heads, n_tp)),
             dma((seqs, n_tp * heads)),
         ],
         compiler_params=pltpu.CompilerParams(
@@ -484,7 +638,8 @@
     heads = head_lambda.shape[0]
     fits = (
         heads == n_sp
-        and n_sp > 1
+        and n_sp == 4
+        and w_out.shape[0] % 16 == 0
         and n_tp % 2 == 0
         and w_query.shape[1] == heads * LANES
         and sub_gain.shape[0] == LANES
@@ -492,7 +647,7 @@
         and (tokens.shape[0] * n_tp) % SPAN == 0
     )
     if fits:
-        return fused_device(n_sp, n_tp, *args)
+        return fused_device(1, n_sp, n_tp, *args)
     return on_device(*args)
 
 

time: 113 us -> 111 us (0.982)
  the two profiles are of different devices: /device:TPU:24 before, /device:TPU:0 now
where the time goes in v2:
time: 111 us; the launch traced here: 110 us
  Pallas kernels  104 us (94%)
  local copies, waits for them, and re-layouts  5.82 us (5%)
    pallas_call x1, Pallas kernels, fused_device(): pl.pallas_call(functools.partial(layer_kernel, n_grp, n_sp, n_tp), out_sh...  104 us
    transpose x1, local copies, waits for them, and re-layouts, fused_device(): return jnp.transpose(out, (1, 0, 2))  3.27 us
    unnamed x1, local copies, waits for them, and re-layouts  2.54 us

profile of v2, /device:TPU:0, one launch (start us, length us, event | category | flops | bytes accessed | tf_op | source)
XLA Modules:
  0.0 110.2 jit_solution(7093510086225543766)
XLA Ops:
  0.0 2.5 %copy.11 = bf16[128,2,2048]{2,0,1:T(8,128)(2,1)} copy(bf16[128,2,2048]{2,1,0:T(2,128)(2,1)} %param.7) | data formatting | bytes 2097152 | tf_op args[0]
  2.5 104.3 %shard_map.73 = bf16[2,128,2048]{2,1,0:T(8,128)(2,1)} custom-call(bf16[2,128,2048]{2,1,0:T(8,128)(2,1)} %bitcast.6, bf16[2048,512]{1,0:T(8,128)(2,1)} %wq_ref.1, bf16[2048,512]{1,0:T(8,128)(2,1)} %wk_ref.1, bf16[2048,512]{1,0:T(8,128)(2,1)} %wv_ref.1, bf16[512,2048]{1,0:T(8,128)(2,1)} %wo_ref.1, f32[4]{0:T(128)} %lam_ref.1, f32[1,128]{1,0:T(1,128)} %bitcast.7), custom_call_target="tpu_custom_call" | custom-call | tf_op jit(solution)/shard_map/pallas_call | solution.py:589
  106.9 3.3 %copy.9 = bf16[128,2,2048]{2,1,0:T(2,128)(2,1)} copy(bf16[128,2,2048]{2,0,1:T(8,128)(2,1)} %bitcast.5) | data formatting | bytes 2097152 | tf_op jit(solution)/shard_map/transpose | solution.py:632
